TPU v7x, 32 devices: a whole 2x2x4 slice. The times are simulated.
32 devices in a mesh: sp: 8 (over z, core), tp: 4 (over y, x).
Axes of the slice: x: 2, y: 2, z: 4, core: 2. Of those that a mesh axis runs over, the one named last changes fastest.
Arguments:
- residual: bfloat16 [896, 2048], P('sp'), may hold values from -1.5 to 1.5
- latent: bfloat16 [896, 512], P('sp'), may hold values from -6 to 6
- rot_key: bfloat16 [896, 64], P('sp'), may hold values from -6 to 6
- latent_norm_scale: float32 [512], replicated, may hold values from 0.1 to 1.9
- query_wide: bfloat16 [896, 3072], P('sp', 'tp'), may hold values from -210 to 210
- query_narrow: bfloat16 [896, 2048], P('sp', 'tp'), may hold values from -210 to 210
- large_key_lift: bfloat16 [512, 2048], P(None, 'tp'), may hold values from -0.25 to 0.25
- large_value_lift: bfloat16 [512, 2048], P(None, 'tp'), may hold values from -0.25 to 0.25
- small_key_lift: bfloat16 [512, 1024], P(None, 'tp'), may hold values from -0.25 to 0.25
- small_value_lift: bfloat16 [512, 1024], P(None, 'tp'), may hold values from -0.25 to 0.25
- out_wide: bfloat16 [2048, 2048], P('tp'), may hold values from -0.5 to 0.5
- out_narrow: bfloat16 [1024, 2048], P('tp'), may hold values from -0.75 to 0.75
- mix_gain: float32 [2048], replicated, may hold values from 0.1 to 1.9
- router_group: bfloat16 [2048, 4], replicated, may hold values from -0.125 to 0.125
- router_expert: bfloat16 [2048, 8], replicated, may hold values from -0.125 to 0.125
- expert_ids: int32 [896, 2], P('sp'), may hold values from 0 to 7, all different within a row; in each aligned block of 112 rows (0 to 111, 112 to 223, ...) at most 56 rows name the same one
- expert_gate_w: bfloat16 [8, 2048, 4096], P('sp', None, 'tp'), may hold values from -0.125 to 0.125
- expert_up_w: bfloat16 [8, 2048, 4096], P('sp', None, 'tp'), may hold values from -0.125 to 0.125
- expert_down_w: bfloat16 [8, 4096, 2048], P('sp', 'tp'), may hold values from -0.375 to 0.375
Outputs:
- updated: bfloat16 [896, 2048], P('sp', 'tp')
Inputs may be any that keep to these rules, and one draw needn't show every extreme that they name: `expert_ids`: each row names two different experts; the rows of one index of sp name no expert more than 56 times, a bound that some expert reaches in some of these blocks.
All inputs are finite; a program needn't handle non-finite values.
Results may differ from a plain program's by a relative error of at most 0.024.
The roundings to bfloat16 on the way count: a program that leaves them out, or rounds other values in their place, can miss the bound.
Values may be sent and summed in bfloat16 or wider, within the bound.
A program may use at most 64 MiB of HBM per device.

v0:
```python
import jax
import jax.numpy as jnp
from jax import lax
from jax.sharding import PartitionSpec as P

PLAIN_KEY_WIDTH = 128
LARGE_VALUE_SIZE = 128
SMALL_HEAD_WIDTH = 64
ROPE = 64


rope_base = 10000.0
epsilon = 1e-06
very_low = -1e30


def angle_table(positions, width):
    frequency = rope_base ** (-jnp.arange(0, width, 2, dtype=jnp.float32) / width)
    return positions.astype(jnp.float32)[:, None] * frequency[None, :]


def rotate(values, angles):
    half_width = values.shape[-1] // 2
    cosine = jnp.cos(angles)
    sine_part = jnp.sin(angles)
    front_half = values[..., :half_width]
    back_half = values[..., half_width:]
    return jnp.concatenate(
        [front_half * cosine - back_half * sine_part, front_half * sine_part + back_half * cosine],
        axis=-1,
    )


def rms_scale(values, gain):
    return values * lax.rsqrt(jnp.mean(values * values, axis=-1, keepdims=True) + epsilon) * gain


def roped_queries(query, plain_width, angles):
    row_count = query.shape[0]
    shaped = query.reshape(row_count, -1, plain_width + ROPE)
    turned = rotate(shaped[..., plain_width:].astype(jnp.float32), angles[:, None, :]).astype(
        jnp.bfloat16
    )
    return jnp.concatenate([shaped[..., :plain_width], turned], axis=-1)


def expand_keys(latent_rows, large_key_lift, large_value_lift, small_key_lift, small_value_lift):
    row_count = latent_rows.shape[0]

    def project(weight, head_width):
        product = jnp.dot(latent_rows, weight, preferred_element_type=jnp.float32).astype(
            jnp.bfloat16
        )
        return product.reshape(row_count, weight.shape[1] // head_width, head_width)

    return (
        project(large_key_lift, PLAIN_KEY_WIDTH),
        project(large_value_lift, LARGE_VALUE_SIZE),
        project(small_key_lift, SMALL_HEAD_WIDTH),
        project(small_value_lift, SMALL_HEAD_WIDTH),
    )


def attend_group(state, queries, plain_width, key_rows, values, key_rot, causal_mask):
    row_peak, weight_sum, summed = state
    score_scale = (plain_width + ROPE) ** (-0.5)
    scores = jnp.einsum(
        "qhd,khd->qhk", queries[..., :plain_width], key_rows, preferred_element_type=jnp.float32
    )
    scores = scores + jnp.einsum(
        "qhd,kd->qhk", queries[..., plain_width:], key_rot, preferred_element_type=jnp.float32
    )
    scores = scores * score_scale
    allowed = causal_mask[:, None, :]
    new_peak = jnp.maximum(row_peak, jnp.max(jnp.where(allowed, scores, very_low), axis=-1))
    weights = jnp.where(allowed, jnp.exp(scores - new_peak[..., None]), 0.0)
    weight_sum = jnp.sum(weights, axis=-1)
    summed = jnp.einsum(
        "qhk,khd->qhd", weights.astype(jnp.bfloat16), values, preferred_element_type=jnp.float32
    )
    return (new_peak, weight_sum, summed)


def shards(
    residual,
    latent,
    rot_key,
    latent_norm_scale,
    query_wide,
    query_narrow,
    large_key_lift,
    large_value_lift,
    small_key_lift,
    small_value_lift,
    out_wide,
    out_narrow,
    mix_gain,
    router_group,
    router_expert,
    expert_ids,
    expert_gate_w,
    expert_up_w,
    expert_down_w,
):
    tok_rows = latent.shape[0]
    positions = lax.axis_index("sp") * tok_rows + jnp.arange(tok_rows, dtype=jnp.int32)
    angles = angle_table(positions, ROPE)
    normed = rms_scale(latent.astype(jnp.float32), latent_norm_scale).astype(jnp.bfloat16)
    key_turned = rotate(rot_key.astype(jnp.float32), angles).astype(jnp.bfloat16)
    wide_queries = roped_queries(query_wide, PLAIN_KEY_WIDTH, angles)
    narrow_queries = roped_queries(query_narrow, SMALL_HEAD_WIDTH, angles)

    def empty_state(head_count, head_width):
        return (
            jnp.full((tok_rows, head_count), very_low, jnp.float32),
            jnp.zeros((tok_rows, head_count), jnp.float32),
            jnp.zeros((tok_rows, head_count, head_width), jnp.float32),
        )

    initial = (
        empty_state(wide_queries.shape[1], LARGE_VALUE_SIZE),
        empty_state(narrow_queries.shape[1], SMALL_HEAD_WIDTH),
    )
    key_set = expand_keys(
        lax.all_gather(normed, "sp", axis=0, tiled=True),
        large_key_lift,
        large_value_lift,
        small_key_lift,
        small_value_lift,
    )
    key_rot = lax.all_gather(key_turned, "sp", axis=0, tiled=True)
    key_positions = jnp.arange(key_rot.shape[0], dtype=jnp.int32)
    causal_mask = positions[:, None] >= key_positions[None, :]
    wide_state = attend_group(
        initial[0], wide_queries, PLAIN_KEY_WIDTH, key_set[0], key_set[1], key_rot, causal_mask
    )
    narrow_state = attend_group(
        initial[1], narrow_queries, SMALL_HEAD_WIDTH, key_set[2], key_set[3], key_rot, causal_mask
    )

    def heads_out(state):
        return (state[2] / state[1][..., None]).astype(jnp.bfloat16).reshape(tok_rows, -1)

    partial_value = jnp.dot(heads_out(wide_state), out_wide, preferred_element_type=jnp.float32)
    partial_value = partial_value + jnp.dot(
        heads_out(narrow_state), out_narrow, preferred_element_type=jnp.float32
    )
    rounded_partial = lax.optimization_barrier(partial_value.astype(jnp.bfloat16)).astype(
        jnp.float32
    )
    attended = lax.psum(rounded_partial.astype(jnp.bfloat16), "tp").astype(jnp.float32)
    mixed = residual.astype(jnp.float32) + attended
    normal_rows = rms_scale(mixed, mix_gain).astype(jnp.bfloat16)
    group_count = router_group.shape[1]
    expert_count = router_expert.shape[1]
    group_prob = jax.nn.softmax(
        jnp.dot(normal_rows, router_group, preferred_element_type=jnp.float32), axis=-1
    )
    logits = jnp.dot(normal_rows, router_expert, preferred_element_type=jnp.float32)
    chosen_group = expert_ids[:, 0] // (expert_count // group_count)
    group_pick = jnp.sum(
        jnp.where(chosen_group[:, None] == jnp.arange(group_count)[None, :], group_prob, 0.0),
        axis=1,
    )
    expert_match = expert_ids[:, :, None] == jnp.arange(expert_count)[None, None, :]
    chosen_logits = jnp.sum(jnp.where(expert_match, logits[:, None, :], 0.0), axis=2)
    gates = group_pick[:, None] * jax.nn.softmax(chosen_logits, axis=-1)
    tp_size = lax.axis_size("tp")
    sp_size = lax.axis_size("sp")
    capacity = tp_size * max(1, 4 * tok_rows // (expert_count * tp_size))
    flat_ids = expert_ids.reshape(-1)
    one_hot = (flat_ids[:, None] == jnp.arange(expert_count)[None, :]).astype(jnp.int32)
    earlier = jnp.cumsum(one_hot, axis=0) - one_hot
    slot_index = jnp.sum(earlier * one_hot, axis=1)
    target = flat_ids * capacity + slot_index
    source_row = jnp.arange(flat_ids.shape[0], dtype=jnp.int32) // 2
    row_of_slot = jnp.zeros((expert_count * capacity,), jnp.int32).at[target].set(source_row)
    slot_used = jnp.zeros((expert_count * capacity,), jnp.bool_).at[target].set(True)
    outgoing = jnp.where(slot_used[:, None], normal_rows[row_of_slot], jnp.zeros((), jnp.bfloat16))
    outgoing = outgoing.reshape(expert_count, capacity, -1)
    expert_rows = lax.all_to_all(outgoing, "sp", split_axis=0, concat_axis=1, tiled=True)
    lead_blocks = 1
    gate_part = jnp.einsum(
        "erd,edf->erf", expert_rows, expert_gate_w, preferred_element_type=jnp.float32
    )
    up_part = jnp.einsum(
        "erd,edf->erf", expert_rows, expert_up_w, preferred_element_type=jnp.float32
    )
    hidden = (jax.nn.silu(gate_part) * up_part).astype(jnp.bfloat16)
    down_part = jnp.einsum(
        "erf,efd->erd", hidden, expert_down_w, preferred_element_type=jnp.float32
    )
    rounded_down = lax.optimization_barrier(down_part.astype(jnp.bfloat16)).astype(jnp.float32)
    expert_out = lax.psum_scatter(
        rounded_down.astype(jnp.bfloat16), "tp", scatter_dimension=2, tiled=True
    )
    column_count = expert_out.shape[2]
    shaped_out = expert_out.reshape(expert_out.shape[0], lead_blocks, sp_size, -1, column_count)
    returned = lax.all_to_all(shaped_out, "sp", split_axis=2, concat_axis=0, tiled=True)
    returned = returned.reshape(expert_count * capacity, column_count)
    picked = returned[target].astype(jnp.float32).reshape(tok_rows, 2, column_count)
    combined = jnp.sum(picked * gates[:, :, None], axis=1)
    own_columns = lax.dynamic_slice_in_dim(
        mixed, lax.axis_index("tp") * column_count, column_count, 1
    )
    return (own_columns + combined).astype(jnp.bfloat16)


def solution(mesh):
    placed = (
        P("sp", None),
        P("sp", None),
        P("sp", None),
        P(),
        P("sp", "tp"),
        P("sp", "tp"),
        P(None, "tp"),
        P(None, "tp"),
        P(None, "tp"),
        P(None, "tp"),
        P("tp", None),
        P("tp", None),
        P(),
        P(),
        P(),
        P("sp", None),
        P("sp", None, "tp"),
        P("sp", None, "tp"),
        P("sp", "tp", None),
    )
    return jax.shard_map(
        shards, mesh=mesh, in_specs=placed, out_specs=P("sp", "tp"), check_vma=False
    )
```

profile of v0, /device:TPU:0, one launch (start us, length us, event | category | flops | bytes accessed | tf_op | source)
XLA Modules:
  0.0 230.2 jit_solution(13567661316674832507)
XLA Ops:
  6.6 0.9 convert_element_type.96
  7.5 1.1 copy.55
  8.6 1.0 copy.69
  9.8 15.7 %all-gather = bf16[8,112,64]{1,2,0:T(8,128)(2,1)S(1)} all-gather(bf16[1,112,64]{1,2,0:T(8,128)(2,1)S(1)} %maximum_bitcast_fusion), channel_id=1, replica_groups=mesh['sp'=8,'tp'=4] {'sp'}, dimensions={0}, use_global_device_ids=true | all-gather | bytes 129024 | tf_op jit(solution)/shard_map/all_gather | solution.py:131
  25.7 1.0 fusion.36
  26.8 1.0 fusion.38
  27.8 16.2 %all_gather.6 = bf16[896,512]{1,0:T(8,128)(2,1)S(1)} all-gather(bf16[112,512]{1,0:T(8,128)(2,1)S(1)} %fusion.38), channel_id=1, replica_groups=mesh['sp'=8,'tp'=4] {'sp'}, dimensions={0}, use_global_device_ids=true | all-gather | bytes 1032192 | tf_op jit(solution)/shard_map/all_gather | solution.py:125
  47.1 0.9 select_reduce_fusion
  52.5 1.1 fusion.12
  55.2 1.3 scatter_custom_fusion.1
  56.5 1.4 scatter_custom_fusion
  58.0 42.1 %all-reduce.3.cloned.1.call-done = bf16[112,2048]{1,0:T(8,128)(2,1)} async-done(((bf16[112,2048]{1,0:T(8,128)(2,1)}), bf16[112,2048]{1,0:T(8,128)(2,1)}) %all-reduce.3.cloned.1.call-update) | async-done | bytes 458768 | tf_op jit(solution)/shard_map/psum | solution.py:151
  100.2 2.3 convert_add_fusion
  102.7 3.2 %gather_fusion = bf16[448,2048]{1,0:T(8,128)(2,1)} fusion(bf16[112,2048]{1,0:T(8,128)(2,1)S(1)} %multiply_convert_fusion.1, s32[1024]{0:T(1024)S(1)} %pad_clamp_fusion.1), kind=kCustom, calls=%fused_computation | custom fusion | bytes 3671808 | tf_op jit(solution)/shard_map/gather | solution.py:179
  105.9 1.8 broadcast_select_fusion
  107.8 47.8 %all_to_all.8 = bf16[8,56,2048]{2,1,0:T(8,128)(2,1)S(1)} all-to-all(bf16[8,56,2048]{2,1,0:T(8,128)(2,1)S(1)} %broadcast_select_fusion), channel_id=1, replica_groups=mesh['sp'=8,'tp'=4] {'sp'}, dimensions={0} | all-to-all | bytes 3670016 | tf_op jit(solution)/shard_map/all_to_all | solution.py:181
  155.6 1.3 copy-done.1
  156.8 3.3 %fusion.4 = f32[448,1024]{1,0:T(8,128)} fusion(bf16[448,2048]{1,0:T(8,128)(2,1)S(1)} %bitcast.98, bf16[1,2048,1024]{2,1,0:T(8,128)(2,1)S(1)} %copy-done.11), kind=kOutput, calls=%fused_computation.8 | convolution fusion | flops 1879048192 | bytes 7864320 | tf_op jit(solution)/shard_map/erd,edf->erf/dot_general | solution.py:183
  160.2 9.8 %fusion.9 = bf16[1,448,2048]{2,1,0:T(8,128)(2,1)} fusion(bf16[1,1024,2048]{2,1,0:T(8,128)(2,1)} %param.37, f32[448,1024]{1,0:T(8,128)} %fusion.4, bf16[448,2048]{1,0:T(8,128)(2,1)} %bitcast.99, bf16[1,2048,1024]{2,1,0:T(8,128)(2,1)} %param.36), kind=kOutput, calls=%fused_computation.11 | convolution fusion | flops 3761766400 | bytes 13893632 | tf_op jit(solution)/shard_map/erf,efd->erd/dot_general | solution.py:190
  171.0 30.2 %reduce-scatter.2.cloned.1.call-done = bf16[1,448,512]{2,1,0:T(8,128)(2,1)} async-done(((bf16[1,448,2048]{2,1,0:T(8,128)(2,1)}), bf16[1,448,512]{2,1,0:T(8,128)(2,1)}) %reduce-scatter.2.cloned.1.call-update) | async-done | bytes 458768 | tf_op jit(solution)/shard_map/reduce_scatter | solution.py:194
  201.2 4.6 %all-to-all-start.1 = ((bf16[1,1,8,56,512]{4,3,1,0,2:T(8,128)(2,1)}), bf16[1,1,8,56,512]{4,3,1,0,2:T(8,128)(2,1)S(1)}, u32[]{:S(2)}, u32[]{:S(2)}) async-start(bf16[1,1,8,56,512]{4,3,1,0,2:T(8,128)(2,1)} %bitcast.106), calls=%async_computation.2 | async-start | bytes 917504 | tf_op jit(solution)/shard_map/all_to_all | solution.py:199
  206.3 13.4 %all-to-all-done.1 = bf16[1,1,8,56,512]{4,3,1,0,2:T(8,128)(2,1)S(1)} async-done(((bf16[1,1,8,56,512]{4,3,1,0,2:T(8,128)(2,1)}), bf16[1,1,8,56,512]{4,3,1,0,2:T(8,128)(2,1)S(1)}, u32[]{:S(2)}, u32[]{:S(2)}) %all-to-all-start.1) | async-done | bytes 458784 | tf_op jit(solution)/shard_map/all_to_all | solution.py:199
  219.7 1.1 gather_fusion.1
  221.7 1.6 add_convert_fusion
  (89 shorter events, 12.1 us)
Async XLA Ops:
  6.5 44.7 %copy-start = (bf16[512,2048]{1,0:T(8,128)(2,1)S(1)}, bf16[512,2048]{1,0:T(8,128)(2,1)}, u32[]{:S(2)}) copy-start(bf16[512,2048]{1,0:T(8,128)(2,1)} %param.29) | copy-start | bytes 6291460
  6.5 37.5 %copy-start.12 = (bf16[512,512]{1,0:T(8,128)(2,1)S(1)}, bf16[512,512]{1,0:T(8,128)(2,1)}, u32[]{:S(2)}) copy-start(bf16[512,512]{1,0:T(8,128)(2,1)} %param.25) | copy-start | bytes 1572868
  6.5 93.6 %all-reduce.3.cloned.1.call-start = ((), (), s32[]{:S(2)}) async-start(), calls=%async_computation.3 | async-start | bytes 917504 | tf_op jit(solution)/shard_map/psum | solution.py:151
  44.8 1.0 copy-start.5
  47.1 1.0 copy-start.6
  47.1 1.4 copy-start.13
  51.3 1.2 copy-start.4
  51.8 1.9 copy-start.9
  51.8 48.4 %copy-start.2 = (bf16[112,2048]{1,0:T(8,128)(2,1)S(1)}, bf16[112,2048]{1,0:T(8,128)(2,1)}, u32[]{:S(2)}) copy-start(bf16[112,2048]{1,0:T(8,128)(2,1)} %param.19) | copy-start | bytes 1376260
  53.6 48.8 %copy-start.10 = (f32[2048]{0:T(1024)S(1)}, f32[2048]{0:T(1024)}, u32[]{:S(2)}) copy-start(f32[2048]{0:T(1024)} %param.31) | copy-start | bytes 24580
  53.7 147.5 %reduce-scatter.2.cloned.1.call-start = ((), (), s32[]{:S(2)}) async-start(), calls=%async_computation.4 | async-start | bytes 2293760 | tf_op jit(solution)/shard_map/reduce_scatter | solution.py:194
  100.2 2.3 %copy-start.3 = (bf16[112,2048]{1,0:T(8,128)(2,1)S(1)}, bf16[112,2048]{1,0:T(8,128)(2,1)}, u32[]{:S(2)}) copy-start(bf16[112,2048]{1,0:T(8,128)(2,1)} %all-reduce.3.cloned.1.call-done) | copy-start | bytes 1376260
  105.9 50.9 %copy-start.11 = (bf16[1,2048,1024]{2,1,0:T(8,128)(2,1)S(1)}, bf16[1,2048,1024]{2,1,0:T(8,128)(2,1)}, u32[]{:S(2)}) copy-start(bf16[1,2048,1024]{2,1,0:T(8,128)(2,1)} %param.35) | copy-start | bytes 12582916
  155.6 1.3 copy-start.1
  170.0 0.8 copy-start.7
  170.0 35.8 %copy-start.8 = (bf16[2048,4]{0,1:T(4,128)(2,1)S(1)}, bf16[2048,4]{0,1:T(4,128)(2,1)}, u32[]{:S(2)}) copy-start(bf16[2048,4]{0,1:T(4,128)(2,1)} %param.32) | copy-start | bytes 49156
  201.2 18.5 %all-to-all-start.1 = ((bf16[1,1,8,56,512]{4,3,1,0,2:T(8,128)(2,1)}), bf16[1,1,8,56,512]{4,3,1,0,2:T(8,128)(2,1)S(1)}, u32[]{:S(2)}, u32[]{:S(2)}) async-start(bf16[1,1,8,56,512]{4,3,1,0,2:T(8,128)(2,1)} %bitcast.106), calls=%async_computation.2 | async-start | bytes 917504 | tf_op jit(solution)/shard_map/all_to_all | solution.py:199
Sparse Core Ops, SparseCore 0:
  53.8 46.3 all-reduce.2
  170.2 30.9 reduce-scatter.1
where the time goes:
time: 231 us; the launch traced here: 230 us
  waiting for transfers between devices  85.8 us (37%)
  blocking collectives  79.8 us (35%)
  matrix products  20.9 us (9%)
  between operations  13.8 us (6%)
  local copies, waits for them, and re-layouts  13.7 us (6%)
  other arithmetic  11.6 us (5%)
  starting transfers between devices  4.66 us (2%)
    all_to_all x1, blocking collectives, shards(): lax.all_to_all(outgoing, 'sp', split_axis=0, concat_axis=1, tiled=True)  47.8 us
    psum x1, waiting for transfers between devices, shards(): lax.psum(rounded_partial.astype(jnp.bfloat16), 'tp').astype(jnp.float32)  42.1 us
    reduce_scatter x1, waiting for transfers between devices, shards(): lax.psum_scatter(rounded_down.astype(jnp.bfloat16), 'tp', scatter_dimensi...  30.2 us
    all_gather x1, blocking collectives, shards(): lax.all_gather(normed, 'sp', axis=0, tiled=True)  16.2 us
    all_gather x1, blocking collectives, shards(): key_rot = lax.all_gather(key_turned, 'sp', axis=0, tiled=True)  15.7 us
    all_to_all x1, waiting for transfers between devices, shards(): lax.all_to_all(shaped_out, 'sp', split_axis=2, concat_axis=0, tiled=True)  13.4 us
    dot_general x1, matrix products, shards(): jnp.einsum('erf,efd->erd', hidden, expert_down_w, preferred_element_type=...  9.82 us
  transfers between devices with their start and end apart: 3, of which 3 were waited for; matrix products, arithmetic and copies ran while one was open for 2% of the time, Pallas kernels for 0%

commit v1 on v0

--- a/solution.py
+++ b/solution.py
@@ -1,6 +1,10 @@
+import functools
+
 import jax
 import jax.numpy as jnp
 from jax import lax
+from jax.experimental import pallas as pl
+from jax.experimental.pallas import tpu as pltpu
 from jax.sharding import PartitionSpec as P
 
 PLAIN_KEY_WIDTH = 128
@@ -79,6 +83,320 @@
         "qhk,khd->qhd", weights.astype(jnp.bfloat16), values, preferred_element_type=jnp.float32
     )
     return (new_peak, weight_sum, summed)
+
+
+MESH = pl.DeviceIdType.MESH
+VMEM_SPEC = pl.BlockSpec(memory_space=pltpu.VMEM)
+
+
+def flipped(index, bits):
+    result, bit = index, 1
+    while bit <= bits:
+        if bits & bit:
+            result = result + bit - 2 * bit * ((index // bit) % 2)
+        bit *= 2
+    return result
+
+
+def peer_of(index, step, count):
+    if count & (count - 1) == 0:
+        return flipped(index, step)
+    return lax.rem(index + step, count)
+
+
+def source_of(index, step, count):
+    if count & (count - 1) == 0:
+        return flipped(index, step)
+    return lax.rem(index + count - step, count)
+
+
+def to(sp, tp):
+    return {"sp": sp, "tp": tp}
+
+
+def greet(partners):
+    barrier = pltpu.get_barrier_semaphore()
+    for partner in partners:
+        pl.semaphore_signal(barrier, inc=1, device_id=partner, device_id_type=MESH)
+    pl.semaphore_wait(barrier, len(partners))
+
+
+def send(src, dst, send_sem, recv_sem, device):
+    copy = pltpu.make_async_remote_copy(
+        src_ref=src,
+        dst_ref=dst,
+        send_sem=send_sem,
+        recv_sem=recv_sem,
+        device_id=device,
+        device_id_type=MESH,
+    )
+    copy.start()
+    return copy
+
+
+def arrival(dst, send_sem, recv_sem, device):
+    pltpu.make_async_remote_copy(
+        src_ref=dst,
+        dst_ref=dst,
+        send_sem=send_sem,
+        recv_sem=recv_sem,
+        device_id=device,
+        device_id_type=MESH,
+    ).wait_recv()
+
+
+def gather_kernel(sp_count, x_ref, out_ref, send_sem, recv_sem):
+    me, column = lax.axis_index("sp"), lax.axis_index("tp")
+    chips = sp_count // 2
+    chip, core = me // 2, me % 2
+    partner = 2 * chip + 1 - core
+    greet(
+        [to(partner, column)]
+        + [to(2 * peer_of(chip, d, chips) + core, column) for d in range(1, chips)]
+    )
+    copies = []
+    for d in range(chips - 1, 0, -1):
+        there = 2 * peer_of(chip, d, chips) + core
+        copies.append(
+            send(x_ref, out_ref.at[me], send_sem.at[d], recv_sem.at[me], to(there, column))
+        )
+    copies.append(
+        send(x_ref, out_ref.at[me], send_sem.at[0], recv_sem.at[me], to(partner, column))
+    )
+    out_ref[me] = x_ref[...]
+    for d in range(1, chips):
+        origin = 2 * source_of(chip, d, chips) + core
+        block = out_ref.at[origin]
+        arrival(block, send_sem.at[chips + d], recv_sem.at[origin], to(partner, column))
+        copies.append(
+            send(block, block, send_sem.at[chips + d], recv_sem.at[origin], to(partner, column))
+        )
+    for d in range(chips):
+        origin = 2 * source_of(chip, d, chips) + 1 - core
+        arrival(
+            out_ref.at[origin], send_sem.at[0], recv_sem.at[origin], to(partner, column)
+        )
+    for copy in copies:
+        copy.wait_send()
+
+
+def mix_kernel(
+    tp_count,
+    part_ref,
+    residual_ref,
+    gain_ref,
+    router_ref,
+    mixed_ref,
+    stats_ref,
+    held,
+    own_stats,
+    held_stats,
+    send_sem,
+    recv_sem,
+):
+    row, me = lax.axis_index("sp"), lax.axis_index("tp")
+    width = mixed_ref.shape[1]
+    greet([to(row, peer_of(me, d, tp_count)) for d in range(1, tp_count)])
+
+    def columns(index):
+        return pl.ds(pl.multiple_of(index * width, width), width)
+
+    copies = []
+    for d in range(1, tp_count):
+        there = peer_of(me, d, tp_count)
+        copies.append(
+            send(
+                part_ref.at[:, columns(there)],
+                held.at[d],
+                send_sem.at[0, d],
+                recv_sem.at[0, d],
+                to(row, there),
+            )
+        )
+    total = residual_ref[:, columns(me)].astype(jnp.float32)
+    total = total + part_ref[:, columns(me)].astype(jnp.float32)
+    for d in range(1, tp_count):
+        arrival(
+            held.at[d],
+            send_sem.at[0, d],
+            recv_sem.at[0, d],
+            to(row, peer_of(me, d, tp_count)),
+        )
+        total = total + held[d].astype(jnp.float32)
+    mixed_ref[...] = total
+    gained = (total * gain_ref[:, columns(me)]).astype(jnp.bfloat16)
+    contract = (((1,), (1,)), ((), ()))
+    router_rows = router_ref.shape[0]
+    own_stats[:router_rows, :] = lax.dot_general(
+        router_ref[:, columns(me)], gained, contract, preferred_element_type=jnp.float32
+    )
+    own_stats[router_rows:, :] = lax.dot_general(
+        jnp.ones((8, width), jnp.float32),
+        total * total,
+        contract,
+        precision=lax.Precision.HIGHEST,
+        preferred_element_type=jnp.float32,
+    )
+    for d in range(1, tp_count):
+        copies.append(
+            send(
+                own_stats,
+                held_stats.at[d],
+                send_sem.at[1, d],
+                recv_sem.at[1, d],
+                to(row, peer_of(me, d, tp_count)),
+            )
+        )
+    stats = own_stats[...]
+    for d in range(1, tp_count):
+        arrival(
+            held_stats.at[d],
+            send_sem.at[1, d],
+            recv_sem.at[1, d],
+            to(row, peer_of(me, d, tp_count)),
+        )
+        stats = stats + held_stats[d]
+    stats_ref[...] = stats
+    for copy in copies:
+        copy.wait_send()
+
+
+def everyone(row, column, sp_count, tp_count):
+    return [to(peer_of(row, d, sp_count), column) for d in range(1, sp_count)] + [
+        to(row, peer_of(column, e, tp_count)) for e in range(1, tp_count)
+    ]
+
+
+def dispatch_kernel(
+    sp_count, tp_count, x_ref, out_ref, line_send, line_recv, plane_send, plane_recv
+):
+    row, column = lax.axis_index("sp"), lax.axis_index("tp")
+    width = x_ref.shape[2]
+    greet(everyone(row, column, sp_count, tp_count))
+
+    def place(origin, part):
+        return out_ref.at[origin, :, pl.ds(pl.multiple_of(part * width, width), width)]
+
+    copies = []
+    for d in range(sp_count - 1, 0, -1):
+        there = peer_of(row, d, sp_count)
+        copies.append(
+            send(
+                x_ref.at[there],
+                place(row, column),
+                line_send.at[d],
+                line_recv.at[d],
+                to(there, column),
+            )
+        )
+    for d in range(sp_count):
+        origin = source_of(row, d, sp_count)
+        block = place(origin, column)
+        if d > 0:
+            arrival(block, line_send.at[d], line_recv.at[d], to(origin, column))
+        source = block if d > 0 else x_ref.at[row]
+        for e in range(1, tp_count):
+            copies.append(
+                send(
+                    source,
+                    block,
+                    plane_send.at[d, e],
+                    plane_recv.at[d, e],
+                    to(row, peer_of(column, e, tp_count)),
+                )
+            )
+        if d == 0:
+            out_ref[row, :, pl.ds(pl.multiple_of(column * width, width), width)] = x_ref[row]
+    for d in range(sp_count):
+        origin = source_of(row, d, sp_count)
+        for e in range(1, tp_count):
+            part = source_of(column, e, tp_count)
+            arrival(
+                place(origin, part),
+                plane_send.at[d, e],
+                plane_recv.at[d, e],
+                to(row, part),
+            )
+    for copy in copies:
+        copy.wait_send()
+
+
+def combine_kernel(
+    sp_count,
+    tp_count,
+    x_ref,
+    out_ref,
+    held,
+    summed,
+    line_send,
+    line_recv,
+    plane_send,
+    plane_recv,
+):
+    row, column = lax.axis_index("sp"), lax.axis_index("tp")
+    width = out_ref.shape[2]
+    greet(everyone(row, column, sp_count, tp_count))
+
+    def columns(part):
+        return pl.ds(pl.multiple_of(part * width, width), width)
+
+    copies = []
+    for d in range(sp_count - 1, -1, -1):
+        owner = peer_of(row, d, sp_count)
+        for e in range(1, tp_count):
+            there = peer_of(column, e, tp_count)
+            copies.append(
+                send(
+                    x_ref.at[owner, :, columns(there)],
+                    held.at[d, e],
+                    plane_send.at[d, e],
+                    plane_recv.at[d, e],
+                    to(row, there),
+                )
+            )
+    for d in range(sp_count - 1, -1, -1):
+        owner = peer_of(row, d, sp_count)
+        total = x_ref[owner, :, columns(column)].astype(jnp.float32)
+        for e in range(1, tp_count):
+            arrival(
+                held.at[d, e],
+                plane_send.at[d, e],
+                plane_recv.at[d, e],
+                to(row, source_of(column, e, tp_count)),
+            )
+            total = total + held[d, e].astype(jnp.float32)
+        if d == 0:
+            out_ref[row] = total.astype(jnp.bfloat16)
+        else:
+            summed[d] = total.astype(jnp.bfloat16)
+            copies.append(
+                send(
+                    summed.at[d],
+                    out_ref.at[row],
+                    line_send.at[d],
+                    line_recv.at[d],
+                    to(owner, column),
+                )
+            )
+    for d in range(1, sp_count):
+        origin = source_of(row, d, sp_count)
+        arrival(out_ref.at[origin], line_send.at[d], line_recv.at[d], to(origin, column))
+    for copy in copies:
+        copy.wait_send()
+
+
+def call(body, out_shape, scratch, collective_id, *operands):
+    many = isinstance(out_shape, (list, tuple))
+    return pl.pallas_call(
+        body,
+        out_shape=out_shape,
+        in_specs=[VMEM_SPEC] * len(operands),
+        out_specs=[VMEM_SPEC] * len(out_shape) if many else VMEM_SPEC,
+        scratch_shapes=scratch,
+        compiler_params=pltpu.CompilerParams(
+            collective_id=collective_id, has_side_effects=True
+        ),
+    )(*operands)
 
 
 def shards(
@@ -121,14 +439,27 @@
         empty_state(wide_queries.shape[1], LARGE_VALUE_SIZE),
         empty_state(narrow_queries.shape[1], SMALL_HEAD_WIDTH),
     )
+    sp_size, tp_size = lax.axis_size("sp"), lax.axis_size("tp")
+    latent_width = latent.shape[1]
+    dma = pltpu.SemaphoreType.DMA
+    packed = jnp.concatenate(
+        [normed, key_turned, jnp.zeros((tok_rows, (-ROPE) % 128), jnp.bfloat16)], axis=1
+    )
+    gathered = call(
+        functools.partial(gather_kernel, sp_size),
+        jax.ShapeDtypeStruct((sp_size,) + packed.shape, jnp.bfloat16),
+        [dma((sp_size,)), dma((sp_size,))],
+        0,
+        packed,
+    ).reshape(sp_size * tok_rows, -1)
     key_set = expand_keys(
-        lax.all_gather(normed, "sp", axis=0, tiled=True),
+        gathered[:, :latent_width],
         large_key_lift,
         large_value_lift,
         small_key_lift,
         small_value_lift,
     )
-    key_rot = lax.all_gather(key_turned, "sp", axis=0, tiled=True)
+    key_rot = gathered[:, latent_width : latent_width + ROPE]
     key_positions = jnp.arange(key_rot.shape[0], dtype=jnp.int32)
     causal_mask = positions[:, None] >= key_positions[None, :]
     wide_state = attend_group(
@@ -145,65 +476,91 @@
     partial_value = partial_value + jnp.dot(
         heads_out(narrow_state), out_narrow, preferred_element_type=jnp.float32
     )
-    rounded_partial = lax.optimization_barrier(partial_value.astype(jnp.bfloat16)).astype(
-        jnp.float32
-    )
-    attended = lax.psum(rounded_partial.astype(jnp.bfloat16), "tp").astype(jnp.float32)
-    mixed = residual.astype(jnp.float32) + attended
-    normal_rows = rms_scale(mixed, mix_gain).astype(jnp.bfloat16)
     group_count = router_group.shape[1]
     expert_count = router_expert.shape[1]
-    group_prob = jax.nn.softmax(
-        jnp.dot(normal_rows, router_group, preferred_element_type=jnp.float32), axis=-1
-    )
-    logits = jnp.dot(normal_rows, router_expert, preferred_element_type=jnp.float32)
+    model_width = residual.shape[1]
+    column_count = model_width // tp_size
+    router_width = group_count + expert_count
+    router_rows = -(-router_width // 16) * 16
+    router = jnp.concatenate([router_group, router_expert], axis=1)
+    router = jnp.pad(router, ((0, 0), (0, router_rows - router_width))).T
+    mixed, stats = call(
+        functools.partial(mix_kernel, tp_size),
+        [
+            jax.ShapeDtypeStruct((tok_rows, column_count), jnp.float32),
+            jax.ShapeDtypeStruct((router_rows + 8, tok_rows), jnp.float32),
+        ],
+        [
+            pltpu.VMEM((tp_size, tok_rows, column_count), jnp.bfloat16),
+            pltpu.VMEM((router_rows + 8, tok_rows), jnp.float32),
+            pltpu.VMEM((tp_size, router_rows + 8, tok_rows), jnp.float32),
+            dma((2, tp_size)),
+            dma((2, tp_size)),
+        ],
+        1,
+        partial_value.astype(jnp.bfloat16),
+        residual,
+        mix_gain[None, :],
+        router,
+    )
+    inverse = lax.rsqrt(stats[router_rows] / model_width + epsilon)
+    own_gain = lax.dynamic_slice_in_dim(
+        mix_gain, lax.axis_index("tp") * column_count, column_count, 0
+    )
+    normal_rows = (mixed * inverse[:, None] * own_gain).astype(jnp.bfloat16)
+    logits_t = stats[:router_width] * inverse
+    group_prob = jax.nn.softmax(logits_t[:group_count], axis=0)
+    logits = logits_t[group_count:]
     chosen_group = expert_ids[:, 0] // (expert_count // group_count)
     group_pick = jnp.sum(
-        jnp.where(chosen_group[:, None] == jnp.arange(group_count)[None, :], group_prob, 0.0),
-        axis=1,
-    )
-    expert_match = expert_ids[:, :, None] == jnp.arange(expert_count)[None, None, :]
-    chosen_logits = jnp.sum(jnp.where(expert_match, logits[:, None, :], 0.0), axis=2)
-    gates = group_pick[:, None] * jax.nn.softmax(chosen_logits, axis=-1)
-    tp_size = lax.axis_size("tp")
-    sp_size = lax.axis_size("sp")
+        jnp.where(jnp.arange(group_count)[:, None] == chosen_group[None, :], group_prob, 0.0),
+        axis=0,
+    )
+    ids = expert_ids.T
+    expert_match = jnp.arange(expert_count)[None, :, None] == ids[:, None, :]
+    chosen_logits = jnp.sum(jnp.where(expert_match, logits[None], 0.0), axis=1)
+    gates = group_pick * jax.nn.softmax(chosen_logits, axis=0)
     capacity = tp_size * max(1, 4 * tok_rows // (expert_count * tp_size))
-    flat_ids = expert_ids.reshape(-1)
-    one_hot = (flat_ids[:, None] == jnp.arange(expert_count)[None, :]).astype(jnp.int32)
-    earlier = jnp.cumsum(one_hot, axis=0) - one_hot
-    slot_index = jnp.sum(earlier * one_hot, axis=1)
-    target = flat_ids * capacity + slot_index
-    source_row = jnp.arange(flat_ids.shape[0], dtype=jnp.int32) // 2
-    row_of_slot = jnp.zeros((expert_count * capacity,), jnp.int32).at[target].set(source_row)
-    slot_used = jnp.zeros((expert_count * capacity,), jnp.bool_).at[target].set(True)
-    outgoing = jnp.where(slot_used[:, None], normal_rows[row_of_slot], jnp.zeros((), jnp.bfloat16))
-    outgoing = outgoing.reshape(expert_count, capacity, -1)
-    expert_rows = lax.all_to_all(outgoing, "sp", split_axis=0, concat_axis=1, tiled=True)
-    lead_blocks = 1
-    gate_part = jnp.einsum(
-        "erd,edf->erf", expert_rows, expert_gate_w, preferred_element_type=jnp.float32
-    )
-    up_part = jnp.einsum(
-        "erd,edf->erf", expert_rows, expert_up_w, preferred_element_type=jnp.float32
-    )
+    slots = expert_count * capacity
+    match = expert_match.astype(jnp.bfloat16)
+    named = match[0] + match[1]
+    before = (jnp.arange(tok_rows)[:, None] < jnp.arange(tok_rows)[None, :]).astype(jnp.bfloat16)
+    earlier = jnp.dot(named, before, preferred_element_type=jnp.float32).astype(jnp.int32)
+    slot_index = jnp.sum(jnp.where(expert_match, earlier[None], 0), axis=1)
+    target = ids * capacity + slot_index
+    pick = (jnp.arange(slots)[None, :, None] == target[:, None, :]).astype(jnp.bfloat16)
+    outgoing = jnp.dot(pick[0] + pick[1], normal_rows, preferred_element_type=jnp.float32)
+    outgoing = outgoing.astype(jnp.bfloat16).reshape(expert_count, capacity, column_count)
+    plane = [dma((sp_size,)), dma((sp_size,)), dma((sp_size, tp_size)), dma((sp_size, tp_size))]
+    expert_rows = call(
+        functools.partial(dispatch_kernel, sp_size, tp_size),
+        jax.ShapeDtypeStruct((sp_size, capacity, model_width), jnp.bfloat16),
+        plane,
+        2,
+        outgoing,
+    ).reshape(sp_size * capacity, model_width)
+    gate_part = jnp.dot(expert_rows, expert_gate_w[0], preferred_element_type=jnp.float32)
+    up_part = jnp.dot(expert_rows, expert_up_w[0], preferred_element_type=jnp.float32)
     hidden = (jax.nn.silu(gate_part) * up_part).astype(jnp.bfloat16)
-    down_part = jnp.einsum(
-        "erf,efd->erd", hidden, expert_down_w, preferred_element_type=jnp.float32
-    )
-    rounded_down = lax.optimization_barrier(down_part.astype(jnp.bfloat16)).astype(jnp.float32)
-    expert_out = lax.psum_scatter(
-        rounded_down.astype(jnp.bfloat16), "tp", scatter_dimension=2, tiled=True
-    )
-    column_count = expert_out.shape[2]
-    shaped_out = expert_out.reshape(expert_out.shape[0], lead_blocks, sp_size, -1, column_count)
-    returned = lax.all_to_all(shaped_out, "sp", split_axis=2, concat_axis=0, tiled=True)
-    returned = returned.reshape(expert_count * capacity, column_count)
-    picked = returned[target].astype(jnp.float32).reshape(tok_rows, 2, column_count)
-    combined = jnp.sum(picked * gates[:, :, None], axis=1)
-    own_columns = lax.dynamic_slice_in_dim(
-        mixed, lax.axis_index("tp") * column_count, column_count, 1
-    )
-    return (own_columns + combined).astype(jnp.bfloat16)
+    down_part = jnp.dot(hidden, expert_down_w[0], preferred_element_type=jnp.float32)
+    returned = call(
+        functools.partial(combine_kernel, sp_size, tp_size),
+        jax.ShapeDtypeStruct((expert_count, capacity, column_count), jnp.bfloat16),
+        [
+            pltpu.VMEM((sp_size, tp_size, capacity, column_count), jnp.bfloat16),
+            pltpu.VMEM((sp_size, capacity, column_count), jnp.bfloat16),
+        ]
+        + plane,
+        3,
+        down_part.astype(jnp.bfloat16).reshape(sp_size, capacity, model_width),
+    ).reshape(slots, column_count)
+    combined = mixed
+    for k in range(2):
+        picked = lax.dot_general(
+            pick[k], returned, (((0,), (0,)), ((), ())), preferred_element_type=jnp.float32
+        )
+        combined = combined + picked * gates[k][:, None]
+    return combined.astype(jnp.bfloat16)
 
 
 def solution(mesh):

time: 231 us -> 136 us (0.59)
  Pallas kernels: 0 us -> 94.8 us
  waiting for transfers between devices: 85.8 us -> 0 us
  blocking collectives: 79.8 us -> 0 us
  between operations: 13.8 us -> 0.32 us
  matrix products: 20.9 us -> 29.6 us
  local copies, waits for them, and re-layouts: 13.7 us -> 5.96 us
  other arithmetic: 11.6 us -> 4.64 us
  starting transfers between devices: 4.66 us -> 0 us
    pallas_call x0 -> x4, Pallas kernels: none -> 94.8 us  [call(): pl.pallas_call(body, out_shape=out_shape, in_specs=[VMEM_SPEC] * len(oper...]
    all_to_all x1 -> x0, blocking collectives: 47.8 us -> none  [shards(): lax.all_to_all(outgoing, 'sp', split_axis=0, concat_axis=1, tiled=True)]
    psum x1 -> x0, waiting for transfers between devices: 42.1 us -> none  [shards(): lax.psum(rounded_partial.astype(jnp.bfloat16), 'tp').astype(jnp.float32)]
    all_gather x2 -> x0, blocking collectives: 31.9 us -> none  [the longest x1 16.2 us: shards(): lax.all_gather(normed, 'sp', axis=0, tiled=True)]
    reduce_scatter x1 -> x0, waiting for transfers between devices: 30.2 us -> none  [shards(): lax.psum_scatter(rounded_down.astype(jnp.bfloat16), 'tp', scatter_dimensi...]
    all_to_all x1 -> x0, waiting for transfers between devices: 13.4 us -> none  [shards(): lax.all_to_all(shaped_out, 'sp', split_axis=2, concat_axis=0, tiled=True)]
    dot_general x4 -> x6, matrix products: 13.6 us -> 21.3 us  [the longest x1 9.79 us: shards(): jnp.dot(hidden, expert_down_w[0], preferred_element_type=jnp.float32)]
    all_to_all x1 -> x0, starting transfers between devices: 4.61 us -> none  [shards(): lax.all_to_all(shaped_out, 'sp', split_axis=2, concat_axis=0, tiled=True)]
  transfers between devices with their start and end apart: 3 -> 0, of which waited for: 3 -> 0; matrix products, arithmetic and copies ran while one was open for 2% -> 0% of each run, Pallas kernels for 0% -> 0%
where the time goes in v1:
time: 136 us; the launch traced here: 135 us
  Pallas kernels  94.8 us (70%)
  matrix products  29.6 us (22%)
  local copies, waits for them, and re-layouts  5.96 us (4%)
  other arithmetic  4.64 us (3%)
    pallas_call x4, Pallas kernels, call(): pl.pallas_call(body, out_shape=out_shape, in_specs=[VMEM_SPEC] * len(oper...  94.8 us
    dot_general x1, matrix products, shards(): jnp.dot(hidden, expert_down_w[0], preferred_element_type=jnp.float32)  9.79 us
    dot_general x1, matrix products, shards(): jnp.dot(expert_rows, expert_gate_w[0], preferred_element_type=jnp.float32)  6.06 us
    unnamed x28, local copies, waits for them, and re-layouts  3.96 us
    dot_general x2, matrix products, shards(): lax.dot_general(pick[k], returned, (((0,), (0,)), ((), ())), preferred_el...  3.24 us

profile of v1, /device:TPU:0, one launch (start us, length us, event | category | flops | bytes accessed | tf_op | source)
XLA Modules:
  0.0 135.3 jit_solution(4008237172392821669)
XLA Ops:
  0.0 1.0 copy.49
  1.4 1.1 copy.51
  2.6 1.0 copy.63
  4.0 0.7 maximum_maximum_fusion.x_ref
  4.7 21.7 %shard_map.181 = bf16[8,112,640]{2,1,0:T(8,128)(2,1)} custom-call(bf16[112,640]{1,0:T(8,128)(2,1)} %maximum_maximum_fusion.x_ref), custom_call_target="tpu_custom_call" | custom-call | tf_op jit(solution)/shard_map/pallas_call | solution.py:390
  26.4 1.5 %fusion.43 = f32[112,4,896]{2,0,1:T(8,128)S(1)} fusion(bf16[896,640]{1,0:T(8,128)(2,1)} %bitcast.110, bf16[112,4,32]{0,2,1:T(8,128)(2,1)S(1)} %get-tuple-element.19, bf16[112,4,32]{0,2,1:T(8,128)(2,1)S(1)} %get-tuple-element.20), kind=kOutput, calls=%fused_computation.61 | convolution fusion | flops 51494912 | bytes 1892352 | tf_op jit(solution)/shard_map/qhd,kd->qhk/dot_general | solution.py:74
  27.9 0.8 convolution_convert_fusion
  30.7 0.8 select_reduce_fusion
  31.5 0.8 fusion.16
  34.0 0.8 convolution_convert_fusion.1
  35.9 0.7 copy-done.2
  36.6 1.1 fusion.9.part_ref
  37.7 0.7 fusion.56.router_ref
  38.4 15.4 %shard_map.182 = (f32[112,512]{1,0:T(8,128)}, f32[24,112]{1,0:T(8,128)}) custom-call(bf16[112,2048]{1,0:T(8,128)(2,1)} %fusion.9.part_ref, bf16[112,2048]{1,0:T(8,128)(2,1)} %residual_ref.1, f32[1,2048]{1,0:T(1,128)} %bitcast.130, bf16[16,2048]{1,0:T(8,128)(2,1)} %fusion.56.router_ref), custom_call_target="tpu_custom_call" | custom-call | tf_op jit(solution)/shard_map/pallas_call | solution.py:390
  53.8 0.7 rsqrt_bitcast_fusion
  54.5 0.7 slice_multiply_fusion
  55.4 0.8 dynamic_slice.3
  56.4 2.0 %convolution_convert_fusion.4 = bf16[448,512]{1,0:T(8,128)(2,1)} fusion(f32[112,512]{1,0:T(8,128)} %get-tuple-element.7, bf16[2,448,112]{2,1,0:T(8,128)(2,1)S(1)} %get-tuple-element.24, f32[512]{0:T(512)S(1)} %dynamic_slice.3, f32[112]{0:T(128)S(1)} %rsqrt_bitcast_fusion), kind=kOutput, calls=%fused_computation.26 | convolution fusion | flops 51831808 | bytes 891328 | tf_op jit(solution)/shard_map/dot_general | solution.py:532
  58.5 27.7 %shard_map.183 = bf16[8,56,2048]{2,1,0:T(8,128)(2,1)} custom-call(bf16[8,56,512]{2,1,0:T(8,128)(2,1)} %bitcast.119), custom_call_target="tpu_custom_call" | custom-call | tf_op jit(solution)/shard_map/pallas_call | solution.py:390
  86.1 6.1 %fusion.4 = f32[448,1024]{1,0:T(8,128)} fusion(bf16[448,2048]{1,0:T(8,128)(2,1)} %bitcast.116, bf16[1,2048,1024]{2,1,0:T(8,128)(2,1)} %param.35), kind=kOutput, calls=%fused_computation.4 | convolution fusion | flops 1879048192 | bytes 7864320 | tf_op jit(solution)/shard_map/dot_general | solution.py:542
  92.2 9.8 %fusion.6 = bf16[448,2048]{1,0:T(8,128)(2,1)} fusion(bf16[1,1024,2048]{2,1,0:T(8,128)(2,1)} %param.37, f32[448,1024]{1,0:T(8,128)} %fusion.4, bf16[448,2048]{1,0:T(8,128)(2,1)} %bitcast.117, bf16[1,2048,1024]{2,1,0:T(8,128)(2,1)} %param.36), kind=kOutput, calls=%fused_computation.6 | convolution fusion | flops 3761766400 | bytes 13893632 | tf_op jit(solution)/shard_map/dot_general | solution.py:545
  102.0 30.1 %shard_map.184 = bf16[8,56,512]{2,1,0:T(8,128)(2,1)} custom-call(bf16[8,56,2048]{2,1,0:T(8,128)(2,1)} %bitcast.118), custom_call_target="tpu_custom_call" | custom-call | tf_op jit(solution)/shard_map/pallas_call | solution.py:390
  132.1 1.3 fusion.19
  133.4 1.9 %fusion.22 = bf16[112,512]{1,0:T(8,128)(2,1)} fusion(f32[112,512]{1,0:T(8,128)S(1)} %fusion.19, bf16[448,512]{1,0:T(8,128)(2,1)} %bitcast.109, pred[2,448,112]{2,1,0:T(32,128)(4,1)S(1)} %get-tuple-element.23, f32[112]{0:T(128)S(1)} %get-tuple-element.21), kind=kOutput, calls=%fused_computation.34 | convolution fusion | flops 51552256 | bytes 860672 | tf_op jit(solution)/shard_map/dot_general | solution.py:559
  (63 shorter events, 5.9 us)
Async XLA Ops:
  0.0 35.4 %copy-start = (bf16[512,2048]{1,0:T(8,128)(2,1)S(1)}, bf16[512,2048]{1,0:T(8,128)(2,1)}, u32[]{:S(2)}) copy-start(bf16[512,2048]{1,0:T(8,128)(2,1)} %param.29) | copy-start | bytes 6291460
  0.0 3.7 %copy-start.4 = (bf16[112,512]{1,0:T(8,128)(2,1)S(1)}, bf16[112,512]{1,0:T(8,128)(2,1)}, u32[]{:S(2)}) copy-start(bf16[112,512]{1,0:T(8,128)(2,1)} %param.20) | copy-start | bytes 344068
  0.0 3.8 %copy-start.8 = (f32[512]{0:T(512)S(1)}, f32[512]{0:T(512)}, u32[]{:S(2)}) copy-start(f32[512]{0:T(512)} %param.22) | copy-start | bytes 6148
  4.7 23.1 %copy-start.9 = (bf16[512,512]{1,0:T(8,128)(2,1)S(1)}, bf16[512,512]{1,0:T(8,128)(2,1)}, u32[]{:S(2)}) copy-start(bf16[512,512]{1,0:T(8,128)(2,1)} %param.25) | copy-start | bytes 1572868
  26.4 1.5 %copy-start.1 = (bf16[8,112,640]{2,1,0:T(8,128)(2,1)S(1)}, bf16[8,112,640]{2,1,0:T(8,128)(2,1)}, u32[]{:S(2)}) copy-start(bf16[8,112,640]{2,1,0:T(8,128)(2,1)} %shard_map.181) | copy-start | bytes 3440644
  28.6 1.0 copy-start.11
  31.5 1.0 copy-start.12
  33.0 1.0 copy-start.10
  35.4 1.2 copy-start.2
  36.6 1.1 copy-start.5
  36.6 1.1 copy-start.6
  36.6 18.6 %copy-start.7 = (s32[112,2]{0,1:T(2,128)S(1)}, s32[112,2]{0,1:T(2,128)}, u32[]{:S(2)}) copy-start(s32[112,2]{0,1:T(2,128)} %param.34) | copy-start | bytes 2692
  102.0 30.1 %copy-start.3 = (f32[112,512]{1,0:T(8,128)S(1)}, f32[112,512]{1,0:T(8,128)}, u32[]{:S(2)}) copy-start(f32[112,512]{1,0:T(8,128)} %get-tuple-element.7) | copy-start | bytes 688132

commit v2 on v1

--- a/solution.py
+++ b/solution.py
@@ -267,38 +267,73 @@
     ]
 
 
-def dispatch_kernel(
-    sp_count, tp_count, x_ref, out_ref, line_send, line_recv, plane_send, plane_recv
+def expert_kernel(
+    sp_count,
+    tp_count,
+    x_ref,
+    gate_hbm,
+    up_hbm,
+    down_hbm,
+    out_ref,
+    rows,
+    part,
+    held,
+    summed,
+    hidden,
+    gate_w,
+    up_w,
+    down_w,
+    load_sem,
+    line_send,
+    line_recv,
+    plane_send,
+    plane_recv,
+    back_send,
+    back_recv,
+    sum_send,
+    sum_recv,
 ):
     row, column = lax.axis_index("sp"), lax.axis_index("tp")
-    width = x_ref.shape[2]
+    capacity, width = x_ref.shape[1:]
+    model_width = part.shape[2]
+    loads = [
+        pltpu.make_async_copy(gate_hbm, gate_w, load_sem.at[0]),
+        pltpu.make_async_copy(up_hbm, up_w, load_sem.at[1]),
+        pltpu.make_async_copy(down_hbm, down_w, load_sem.at[2]),
+    ]
+    for load in loads:
+        load.start()
     greet(everyone(row, column, sp_count, tp_count))
 
-    def place(origin, part):
-        return out_ref.at[origin, :, pl.ds(pl.multiple_of(part * width, width), width)]
+    def columns(index):
+        return pl.ds(pl.multiple_of(index * width, width), width)
 
     copies = []
-    for d in range(sp_count - 1, 0, -1):
+    for d in range(1, sp_count):
         there = peer_of(row, d, sp_count)
         copies.append(
             send(
                 x_ref.at[there],
-                place(row, column),
+                rows.at[d, :, columns(column)],
                 line_send.at[d],
                 line_recv.at[d],
                 to(there, column),
             )
         )
-    for d in range(sp_count):
-        origin = source_of(row, d, sp_count)
-        block = place(origin, column)
+
+    def spread(d):
+        block = rows.at[d, :, columns(column)]
         if d > 0:
-            arrival(block, line_send.at[d], line_recv.at[d], to(origin, column))
-        source = block if d > 0 else x_ref.at[row]
+            arrival(
+                block,
+                line_send.at[d],
+                line_recv.at[d],
+                to(source_of(row, d, sp_count), column),
+            )
         for e in range(1, tp_count):
             copies.append(
                 send(
-                    source,
+                    block if d > 0 else x_ref.at[row],
                     block,
                     plane_send.at[d, e],
                     plane_recv.at[d, e],
@@ -306,91 +341,111 @@
                 )
             )
         if d == 0:
-            out_ref[row, :, pl.ds(pl.multiple_of(column * width, width), width)] = x_ref[row]
-    for d in range(sp_count):
-        origin = source_of(row, d, sp_count)
-        for e in range(1, tp_count):
-            part = source_of(column, e, tp_count)
-            arrival(
-                place(origin, part),
-                plane_send.at[d, e],
-                plane_recv.at[d, e],
-                to(row, part),
-            )
-    for copy in copies:
-        copy.wait_send()
-
-
-def combine_kernel(
-    sp_count,
-    tp_count,
-    x_ref,
-    out_ref,
-    held,
-    summed,
-    line_send,
-    line_recv,
-    plane_send,
-    plane_recv,
-):
-    row, column = lax.axis_index("sp"), lax.axis_index("tp")
-    width = out_ref.shape[2]
-    greet(everyone(row, column, sp_count, tp_count))
-
-    def columns(part):
-        return pl.ds(pl.multiple_of(part * width, width), width)
-
-    copies = []
-    for d in range(sp_count - 1, -1, -1):
-        owner = peer_of(row, d, sp_count)
-        for e in range(1, tp_count):
-            there = peer_of(column, e, tp_count)
-            copies.append(
-                send(
-                    x_ref.at[owner, :, columns(there)],
-                    held.at[d, e],
+            rows[0, :, columns(column)] = x_ref[row]
+
+    def run(first, count):
+        for d in range(first, first + count):
+            for e in range(1, tp_count):
+                origin = source_of(column, e, tp_count)
+                arrival(
+                    rows.at[d, :, columns(origin)],
                     plane_send.at[d, e],
                     plane_recv.at[d, e],
-                    to(row, there),
+                    to(row, origin),
                 )
-            )
-    for d in range(sp_count - 1, -1, -1):
-        owner = peer_of(row, d, sp_count)
-        total = x_ref[owner, :, columns(column)].astype(jnp.float32)
+        tall = count * capacity
+        if first == 0:
+            loads[0].wait()
+            loads[1].wait()
+        unit_tile = min(256, hidden.shape[1])
+
+        def units(n, carry):
+            here = pl.ds(pl.multiple_of(n * unit_tile, unit_tile), unit_tile)
+            tokens = rows[first : first + count].reshape(tall, model_width)
+            gate = jnp.dot(tokens, gate_w[:, here], preferred_element_type=jnp.float32)
+            up = jnp.dot(tokens, up_w[:, here], preferred_element_type=jnp.float32)
+            hidden[:, here] = (gate / (1.0 + jnp.exp(-gate)) * up).astype(jnp.bfloat16)
+            return carry
+
+        lax.fori_loop(0, hidden.shape[1] // unit_tile, units, 0)
+        if first == 0:
+            loads[2].wait()
+        tile = min(256, model_width)
+
+        def outputs(n, carry):
+            here = pl.ds(pl.multiple_of(n * tile, tile), tile)
+            product = jnp.dot(hidden[...], down_w[:, here], preferred_element_type=jnp.float32)
+            part[first : first + count, :, here] = product.astype(jnp.bfloat16).reshape(
+                count, capacity, tile
+            )
+            return carry
+
+        lax.fori_loop(0, model_width // tile, outputs, 0)
+        for d in range(first, first + count):
+            for e in range(1, tp_count):
+                there = peer_of(column, e, tp_count)
+                copies.append(
+                    send(
+                        part.at[d, :, columns(there)],
+                        held.at[d, e],
+                        back_send.at[d, e],
+                        back_recv.at[d, e],
+                        to(row, there),
+                    )
+                )
+
+    def finish(d):
+        total = part[d, :, columns(column)].astype(jnp.float32)
         for e in range(1, tp_count):
             arrival(
                 held.at[d, e],
-                plane_send.at[d, e],
-                plane_recv.at[d, e],
+                back_send.at[d, e],
+                back_recv.at[d, e],
                 to(row, source_of(column, e, tp_count)),
             )
             total = total + held[d, e].astype(jnp.float32)
         if d == 0:
             out_ref[row] = total.astype(jnp.bfloat16)
         else:
+            owner = source_of(row, d, sp_count)
             summed[d] = total.astype(jnp.bfloat16)
             copies.append(
                 send(
                     summed.at[d],
                     out_ref.at[row],
-                    line_send.at[d],
-                    line_recv.at[d],
+                    sum_send.at[d],
+                    sum_recv.at[d],
                     to(owner, column),
                 )
             )
+
+    count = 2
+    for d in range(count):
+        spread(d)
+    for first in range(0, sp_count, count):
+        if first + count < sp_count:
+            for d in range(first + count, first + 2 * count):
+                spread(d)
+        run(first, count)
+        if first > 0:
+            for d in range(first - count, first):
+                finish(d)
+    for d in range(sp_count - count, sp_count):
+        finish(d)
     for d in range(1, sp_count):
-        origin = source_of(row, d, sp_count)
-        arrival(out_ref.at[origin], line_send.at[d], line_recv.at[d], to(origin, column))
+        expert = peer_of(row, d, sp_count)
+        arrival(out_ref.at[expert], sum_send.at[d], sum_recv.at[d], to(expert, column))
     for copy in copies:
         copy.wait_send()
 
 
-def call(body, out_shape, scratch, collective_id, *operands):
+def call(body, out_shape, scratch, collective_id, *operands, streamed=0):
     many = isinstance(out_shape, (list, tuple))
     return pl.pallas_call(
         body,
         out_shape=out_shape,
-        in_specs=[VMEM_SPEC] * len(operands),
+        in_specs=[VMEM_SPEC] * (len(operands) - streamed)
+        + [pl.BlockSpec(memory_space=pl.ANY)] * streamed,
         out_specs=[VMEM_SPEC] * len(out_shape) if many else VMEM_SPEC,
         scratch_shapes=scratch,
         compiler_params=pltpu.CompilerParams(
@@ -531,28 +586,37 @@
     pick = (jnp.arange(slots)[None, :, None] == target[:, None, :]).astype(jnp.bfloat16)
     outgoing = jnp.dot(pick[0] + pick[1], normal_rows, preferred_element_type=jnp.float32)
     outgoing = outgoing.astype(jnp.bfloat16).reshape(expert_count, capacity, column_count)
-    plane = [dma((sp_size,)), dma((sp_size,)), dma((sp_size, tp_size)), dma((sp_size, tp_size))]
-    expert_rows = call(
-        functools.partial(dispatch_kernel, sp_size, tp_size),
-        jax.ShapeDtypeStruct((sp_size, capacity, model_width), jnp.bfloat16),
-        plane,
+    line, plane = dma((sp_size,)), dma((sp_size, tp_size))
+    units = expert_down_w.shape[1]
+    bf16 = jnp.bfloat16
+    returned = call(
+        functools.partial(expert_kernel, sp_size, tp_size),
+        jax.ShapeDtypeStruct((expert_count, capacity, column_count), bf16),
+        [
+            pltpu.VMEM((sp_size, capacity, model_width), bf16),
+            pltpu.VMEM((sp_size, capacity, model_width), bf16),
+            pltpu.VMEM((sp_size, tp_size, capacity, column_count), bf16),
+            pltpu.VMEM((sp_size, capacity, column_count), bf16),
+            pltpu.VMEM((2 * capacity, units), bf16),
+            pltpu.VMEM((model_width, units), bf16),
+            pltpu.VMEM((model_width, units), bf16),
+            pltpu.VMEM((units, model_width), bf16),
+            dma((3,)),
+            line,
+            line,
+            plane,
+            plane,
+            plane,
+            plane,
+            line,
+            line,
+        ],
         2,
         outgoing,
-    ).reshape(sp_size * capacity, model_width)
-    gate_part = jnp.dot(expert_rows, expert_gate_w[0], preferred_element_type=jnp.float32)
-    up_part = jnp.dot(expert_rows, expert_up_w[0], preferred_element_type=jnp.float32)
-    hidden = (jax.nn.silu(gate_part) * up_part).astype(jnp.bfloat16)
-    down_part = jnp.dot(hidden, expert_down_w[0], preferred_element_type=jnp.float32)
-    returned = call(
-        functools.partial(combine_kernel, sp_size, tp_size),
-        jax.ShapeDtypeStruct((expert_count, capacity, column_count), jnp.bfloat16),
-        [
-            pltpu.VMEM((sp_size, tp_size, capacity, column_count), jnp.bfloat16),
-            pltpu.VMEM((sp_size, capacity, column_count), jnp.bfloat16),
-        ]
-        + plane,
-        3,
-        down_part.astype(jnp.bfloat16).reshape(sp_size, capacity, model_width),
+        expert_gate_w[0],
+        expert_up_w[0],
+        expert_down_w[0],
+        streamed=3,
     ).reshape(slots, column_count)
     combined = mixed
     for k in range(2):

time: 136 us -> 115 us (0.85)
  matrix products: 29.6 us -> 13.8 us
  Pallas kernels: 94.8 us -> 88.9 us
    dot_general x2 -> x0, matrix products: 15.9 us -> none  [the longest x1 9.79 us: shards(): jnp.dot(hidden, expert_down_w[0], preferred_element_type=jnp.float32)]
    pallas_call x4 -> x3, Pallas kernels: 94.8 us -> 88.9 us  [call(): pl.pallas_call(body, out_shape=out_shape, in_specs=[VMEM_SPEC] * (len(ope...]
where the time goes in v2:
time: 115 us; the launch traced here: 114 us
  Pallas kernels  88.9 us (77%)
  matrix products  13.8 us (12%)
  local copies, waits for them, and re-layouts  5.97 us (5%)
  other arithmetic  4.63 us (4%)
    pallas_call x3, Pallas kernels, call(): pl.pallas_call(body, out_shape=out_shape, in_specs=[VMEM_SPEC] * (len(ope...  88.9 us
    unnamed x28, local copies, waits for them, and re-layouts  3.97 us
    dot_general x2, matrix products, shards(): lax.dot_general(pick[k], returned, (((0,), (0,)), ((), ())), preferred_el...  3.24 us
    dot_general x4, matrix products, project(): jnp.dot(latent_rows, weight, preferred_element_type=jnp.float32)  2.51 us

profile of v2, /device:TPU:0, one launch (start us, length us, event | category | flops | bytes accessed | tf_op | source)
XLA Modules:
  0.0 113.6 jit_solution(15952282013785251125)
XLA Ops:
  0.0 1.0 copy.49
  1.4 1.1 copy.51
  2.6 1.0 copy.63
  4.0 0.7 maximum_maximum_fusion.x_ref
  4.7 21.7 %shard_map.181 = bf16[8,112,640]{2,1,0:T(8,128)(2,1)} custom-call(bf16[112,640]{1,0:T(8,128)(2,1)} %maximum_maximum_fusion.x_ref), custom_call_target="tpu_custom_call" | custom-call | tf_op jit(solution)/shard_map/pallas_call | solution.py:444
  26.4 1.5 %fusion.30 = f32[112,4,896]{2,0,1:T(8,128)S(1)} fusion(bf16[896,640]{1,0:T(8,128)(2,1)} %bitcast.97, bf16[112,4,32]{0,2,1:T(8,128)(2,1)S(1)} %get-tuple-element.19, bf16[112,4,32]{0,2,1:T(8,128)(2,1)S(1)} %get-tuple-element.20), kind=kOutput, calls=%fused_computation.53 | convolution fusion | flops 51494912 | bytes 1892352 | tf_op jit(solution)/shard_map/qhd,kd->qhk/dot_general | solution.py:74
  27.9 0.8 convolution_convert_fusion
  29.1 0.5 copy-done.11
  30.7 0.8 select_reduce_fusion
  31.5 0.8 fusion.5
  33.0 0.5 fusion.14
  34.0 0.8 convolution_convert_fusion.1
  34.8 0.6 fusion.13
  35.9 0.7 copy-done.2
  36.6 1.1 fusion.part_ref
  37.7 0.7 fusion.43.router_ref
  38.4 15.4 %shard_map.182 = (f32[112,512]{1,0:T(8,128)}, f32[24,112]{1,0:T(8,128)}) custom-call(bf16[112,2048]{1,0:T(8,128)(2,1)} %fusion.part_ref, bf16[112,2048]{1,0:T(8,128)(2,1)} %residual_ref.1, f32[1,2048]{1,0:T(1,128)} %bitcast.114, bf16[16,2048]{1,0:T(8,128)(2,1)} %fusion.43.router_ref), custom_call_target="tpu_custom_call" | custom-call | tf_op jit(solution)/shard_map/pallas_call | solution.py:444
  53.8 0.7 rsqrt_bitcast_fusion
  54.5 0.7 slice_multiply_fusion
  55.4 0.8 dynamic_slice.3
  56.4 2.1 %convolution_convert_fusion.4 = bf16[448,512]{1,0:T(8,128)(2,1)} fusion(f32[112,512]{1,0:T(8,128)} %get-tuple-element.7, bf16[2,448,112]{2,1,0:T(8,128)(2,1)S(1)} %get-tuple-element.24, f32[512]{0:T(512)S(1)} %dynamic_slice.3, f32[112]{0:T(128)S(1)} %rsqrt_bitcast_fusion), kind=kOutput, calls=%fused_computation.18 | convolution fusion | flops 51831808 | bytes 891328 | tf_op jit(solution)/shard_map/dot_general | solution.py:587
  58.5 51.9 %shard_map.183 = bf16[8,56,512]{2,1,0:T(8,128)(2,1)} custom-call(bf16[8,56,512]{2,1,0:T(8,128)(2,1)} %bitcast.103, bf16[2048,1024]{1,0:T(8,128)(2,1)} %bitcast.92, bf16[2048,1024]{1,0:T(8,128)(2,1)} %bitcast.93, bf16[1024,2048]{1,0:T(8,128)(2,1)} %bitcast.94), custom_call_target="tpu_custom_call" | custom-call | tf_op jit(solution)/shard_map/pallas_call | solution.py:444
  110.4 1.3 %fusion.8 = f32[112,512]{1,0:T(8,128)S(1)} fusion(f32[112,512]{1,0:T(8,128)S(1)} %copy-done.3, bf16[448,512]{1,0:T(8,128)(2,1)} %bitcast.95, pred[2,448,112]{2,1,0:T(32,128)(4,1)S(1)} %get-tuple-element.23, f32[112]{0:T(128)S(1)} %get-tuple-element.22), kind=kOutput, calls=%fused_computation.22 | convolution fusion | flops 51494912 | bytes 975360 | tf_op jit(solution)/shard_map/dot_general | solution.py:623
  111.7 1.9 %fusion.11 = bf16[112,512]{1,0:T(8,128)(2,1)} fusion(f32[112,512]{1,0:T(8,128)S(1)} %fusion.8, bf16[448,512]{1,0:T(8,128)(2,1)} %bitcast.96, pred[2,448,112]{2,1,0:T(32,128)(4,1)S(1)} %get-tuple-element.23, f32[112]{0:T(128)S(1)} %get-tuple-element.21), kind=kOutput, calls=%fused_computation.26 | convolution fusion | flops 51552256 | bytes 860672 | tf_op jit(solution)/shard_map/dot_general | solution.py:623
  (60 shorter events, 4.3 us)
Async XLA Ops:
  0.0 35.4 %copy-start = (bf16[512,2048]{1,0:T(8,128)(2,1)S(1)}, bf16[512,2048]{1,0:T(8,128)(2,1)}, u32[]{:S(2)}) copy-start(bf16[512,2048]{1,0:T(8,128)(2,1)} %param.29) | copy-start | bytes 6291460
  0.0 3.7 %copy-start.4 = (bf16[112,512]{1,0:T(8,128)(2,1)S(1)}, bf16[112,512]{1,0:T(8,128)(2,1)}, u32[]{:S(2)}) copy-start(bf16[112,512]{1,0:T(8,128)(2,1)} %param.20) | copy-start | bytes 344068
  0.0 3.8 %copy-start.8 = (f32[512]{0:T(512)S(1)}, f32[512]{0:T(512)}, u32[]{:S(2)}) copy-start(f32[512]{0:T(512)} %param.22) | copy-start | bytes 6148
  4.7 23.1 %copy-start.9 = (bf16[512,512]{1,0:T(8,128)(2,1)S(1)}, bf16[512,512]{1,0:T(8,128)(2,1)}, u32[]{:S(2)}) copy-start(bf16[512,512]{1,0:T(8,128)(2,1)} %param.25) | copy-start | bytes 1572868
  26.4 1.5 %copy-start.1 = (bf16[8,112,640]{2,1,0:T(8,128)(2,1)S(1)}, bf16[8,112,640]{2,1,0:T(8,128)(2,1)}, u32[]{:S(2)}) copy-start(bf16[8,112,640]{2,1,0:T(8,128)(2,1)} %shard_map.181) | copy-start | bytes 3440644
  28.6 1.0 copy-start.11
  31.5 1.0 copy-start.12
  33.0 1.0 copy-start.10
  35.4 1.2 %copy-start.2 = (bf16[256,2048]{1,0:T(8,128)(2,1)S(1)}, bf16[256,2048]{1,0:T(8,128)(2,1)}, u32[]{:S(2)}) copy-start(bf16[256,2048]{1,0:T(8,128)(2,1)} %param.30) | copy-start | bytes 3145732
  36.6 1.1 copy-start.5
  36.6 1.1 copy-start.6
  36.6 18.6 %copy-start.7 = (s32[112,2]{0,1:T(2,128)S(1)}, s32[112,2]{0,1:T(2,128)}, u32[]{:S(2)}) copy-start(s32[112,2]{0,1:T(2,128)} %param.34) | copy-start | bytes 2692
  58.4 51.9 %copy-start.3 = (f32[112,512]{1,0:T(8,128)S(1)}, f32[112,512]{1,0:T(8,128)}, u32[]{:S(2)}) copy-start(f32[112,512]{1,0:T(8,128)} %get-tuple-element.7) | copy-start | bytes 688132

commit v3 on v2

--- a/solution.py
+++ b/solution.py
@@ -187,6 +187,7 @@
     gain_ref,
     router_ref,
     mixed_ref,
+    gained_ref,
     stats_ref,
     held,
     own_stats,
@@ -224,7 +225,8 @@
         )
         total = total + held[d].astype(jnp.float32)
     mixed_ref[...] = total
-    gained = (total * gain_ref[:, columns(me)]).astype(jnp.bfloat16)
+    gained_ref[...] = total * gain_ref[:, columns(me)]
+    gained = gained_ref[...].astype(jnp.bfloat16)
     contract = (((1,), (1,)), ((), ()))
     router_rows = router_ref.shape[0]
     own_stats[:router_rows, :] = lax.dot_general(
@@ -539,9 +541,10 @@
     router_rows = -(-router_width // 16) * 16
     router = jnp.concatenate([router_group, router_expert], axis=1)
     router = jnp.pad(router, ((0, 0), (0, router_rows - router_width))).T
-    mixed, stats = call(
+    mixed, gained, stats = call(
         functools.partial(mix_kernel, tp_size),
         [
+            jax.ShapeDtypeStruct((tok_rows, column_count), jnp.float32),
             jax.ShapeDtypeStruct((tok_rows, column_count), jnp.float32),
             jax.ShapeDtypeStruct((router_rows + 8, tok_rows), jnp.float32),
         ],
@@ -559,10 +562,7 @@
         router,
     )
     inverse = lax.rsqrt(stats[router_rows] / model_width + epsilon)
-    own_gain = lax.dynamic_slice_in_dim(
-        mix_gain, lax.axis_index("tp") * column_count, column_count, 0
-    )
-    normal_rows = (mixed * inverse[:, None] * own_gain).astype(jnp.bfloat16)
+    normal_rows = (gained * inverse[:, None]).astype(jnp.bfloat16)
     logits_t = stats[:router_width] * inverse
     group_prob = jax.nn.softmax(logits_t[:group_count], axis=0)
     logits = logits_t[group_count:]
@@ -618,12 +618,11 @@
         expert_down_w[0],
         streamed=3,
     ).reshape(slots, column_count)
-    combined = mixed
-    for k in range(2):
-        picked = lax.dot_general(
-            pick[k], returned, (((0,), (0,)), ((), ())), preferred_element_type=jnp.float32
-        )
-        combined = combined + picked * gates[k][:, None]
+    back = (target[:, :, None] == jnp.arange(slots)[None, None, :]).astype(bf16)
+    picked = jnp.dot(
+        back.reshape(2 * tok_rows, slots), returned, preferred_element_type=jnp.float32
+    ).reshape(2, tok_rows, column_count)
+    combined = mixed + jnp.sum(picked * gates[:, :, None], axis=0)
     return combined.astype(jnp.bfloat16)
 
 

time: 115 us -> 113 us (0.983)
  matrix products: 13.8 us -> 11.9 us
    dot_general x2 -> x1, matrix products: 3.24 us -> 1.38 us  [shards(): jnp.dot(back.reshape(2 * tok_rows, slots), returned, preferred_element_ty...]
where the time goes in v3:
time: 113 us; the launch traced here: 112 us
  Pallas kernels  89 us (79%)
  matrix products  11.9 us (11%)
  other arithmetic  5.27 us (5%)
  local copies, waits for them, and re-layouts  5.2 us (5%)
    pallas_call x3, Pallas kernels, call(): pl.pallas_call(body, out_shape=out_shape, in_specs=[VMEM_SPEC] * (len(ope...  89 us
    unnamed x28, local copies, waits for them, and re-layouts  3.97 us
    dot_general x4, matrix products, project(): jnp.dot(latent_rows, weight, preferred_element_type=jnp.float32)  2.51 us
    dot_general x2, matrix products, attend_group(): jnp.einsum('qhd,kd->qhk', queries[..., plain_width:], key_rot, preferred_...  2.3 us

profile of v3, /device:TPU:0, one launch (start us, length us, event | category | flops | bytes accessed | tf_op | source)
XLA Modules:
  0.0 111.7 jit_solution(14406239301258600135)
XLA Ops:
  0.0 1.0 copy.49
  1.4 1.1 copy.51
  2.6 1.0 copy.63
  4.0 0.7 maximum_maximum_fusion.x_ref
  4.7 21.7 %shard_map.181 = bf16[8,112,640]{2,1,0:T(8,128)(2,1)} custom-call(bf16[112,640]{1,0:T(8,128)(2,1)} %maximum_maximum_fusion.x_ref), custom_call_target="tpu_custom_call" | custom-call | tf_op jit(solution)/shard_map/pallas_call | solution.py:446
  26.4 1.5 %fusion.32 = f32[112,4,896]{2,0,1:T(8,128)S(1)} fusion(bf16[896,640]{1,0:T(8,128)(2,1)} %bitcast.89, bf16[112,4,32]{0,2,1:T(8,128)(2,1)S(1)} %get-tuple-element.21, bf16[112,4,32]{0,2,1:T(8,128)(2,1)S(1)} %get-tuple-element.22), kind=kOutput, calls=%fused_computation.53 | convolution fusion | flops 51494912 | bytes 1892352 | tf_op jit(solution)/shard_map/qhd,kd->qhk/dot_general | solution.py:74
  27.9 0.8 convolution_convert_fusion
  29.1 0.5 copy-done.11
  29.6 0.5 convolution_convert_fusion.2
  30.6 0.8 select_reduce_fusion
  31.5 0.8 fusion.5
  33.0 0.5 fusion.12
  34.0 0.8 convolution_convert_fusion.1
  34.8 0.6 fusion.11
  35.9 0.7 copy-done.2
  36.6 1.1 fusion.part_ref
  37.7 0.7 fusion.44.router_ref
  38.4 15.5 %shard_map.182 = (f32[112,512]{1,0:T(8,128)}, f32[112,512]{1,0:T(8,128)}, f32[24,112]{1,0:T(8,128)}) custom-call(bf16[112,2048]{1,0:T(8,128)(2,1)} %fusion.part_ref, bf16[112,2048]{1,0:T(8,128)(2,1)} %residual_ref.1, f32[1,2048]{1,0:T(1,128)} %bitcast.107, bf16[16,2048]{1,0:T(8,128)(2,1)} %fusion.44.router_ref), custom_call_target="tpu_custom_call" | custom-call | tf_op jit(solution)/shard_map/pallas_call | solution.py:446
  53.8 0.7 rsqrt_bitcast_fusion
  54.5 0.7 slice_multiply_fusion
  55.6 2.0 %convolution_convert_fusion.4 = bf16[448,512]{1,0:T(8,128)(2,1)} fusion(f32[112,512]{1,0:T(8,128)} %get-tuple-element.9, bf16[2,448,112]{2,1,0:T(8,128)(2,1)S(1)} %fusion.27, f32[112]{0:T(128)S(1)} %rsqrt_bitcast_fusion), kind=kOutput, calls=%fused_computation.18 | convolution fusion | flops 51774464 | bytes 889280 | tf_op jit(solution)/shard_map/dot_general | solution.py:587
  57.7 51.9 %shard_map.183 = bf16[8,56,512]{2,1,0:T(8,128)(2,1)} custom-call(bf16[8,56,512]{2,1,0:T(8,128)(2,1)} %bitcast.95, bf16[2048,1024]{1,0:T(8,128)(2,1)} %bitcast.86, bf16[2048,1024]{1,0:T(8,128)(2,1)} %bitcast.87, bf16[1024,2048]{1,0:T(8,128)(2,1)} %bitcast.88), custom_call_target="tpu_custom_call" | custom-call | tf_op jit(solution)/shard_map/pallas_call | solution.py:446
  109.6 1.4 %fusion.7 = f32[112,512]{1,0:T(8,128)S(1)} fusion(bf16[448,512,1]{1,0,2:T(8,128)(2,1)} %bitcast.101, f32[2,112]{1,0:T(2,128)S(1)} %divide_multiply_fusion, s32[2,112]{1,0:T(2,128)S(1)} %multiply_add_fusion), kind=kOutput, calls=%fused_computation.20 | convolution fusion | flops 103032832 | bytes 689920 | tf_op jit(solution)/shard_map/dot_general | solution.py:622
  111.0 0.7 add_convert_fusion
  (58 shorter events, 3.8 us)
Async XLA Ops:
  0.0 35.4 %copy-start = (bf16[512,2048]{1,0:T(8,128)(2,1)S(1)}, bf16[512,2048]{1,0:T(8,128)(2,1)}, u32[]{:S(2)}) copy-start(bf16[512,2048]{1,0:T(8,128)(2,1)} %param.29) | copy-start | bytes 6291460
  0.0 3.7 %copy-start.3 = (bf16[112,512]{1,0:T(8,128)(2,1)S(1)}, bf16[112,512]{1,0:T(8,128)(2,1)}, u32[]{:S(2)}) copy-start(bf16[112,512]{1,0:T(8,128)(2,1)} %param.20) | copy-start | bytes 344068
  0.0 3.8 %copy-start.8 = (f32[512]{0:T(512)S(1)}, f32[512]{0:T(512)}, u32[]{:S(2)}) copy-start(f32[512]{0:T(512)} %param.22) | copy-start | bytes 6148
  4.7 23.1 %copy-start.9 = (bf16[512,512]{1,0:T(8,128)(2,1)S(1)}, bf16[512,512]{1,0:T(8,128)(2,1)}, u32[]{:S(2)}) copy-start(bf16[512,512]{1,0:T(8,128)(2,1)} %param.25) | copy-start | bytes 1572868
  26.4 1.5 %copy-start.1 = (bf16[8,112,640]{2,1,0:T(8,128)(2,1)S(1)}, bf16[8,112,640]{2,1,0:T(8,128)(2,1)}, u32[]{:S(2)}) copy-start(bf16[8,112,640]{2,1,0:T(8,128)(2,1)} %shard_map.181) | copy-start | bytes 3440644
  28.6 1.0 copy-start.11
  31.5 1.0 copy-start.12
  33.0 1.0 copy-start.10
  35.4 1.2 %copy-start.2 = (bf16[256,2048]{1,0:T(8,128)(2,1)S(1)}, bf16[256,2048]{1,0:T(8,128)(2,1)}, u32[]{:S(2)}) copy-start(bf16[256,2048]{1,0:T(8,128)(2,1)} %param.30) | copy-start | bytes 3145732
  36.6 1.1 copy-start.5
  36.6 1.1 copy-start.6
  36.6 18.7 %copy-start.7 = (s32[112,2]{0,1:T(2,128)S(1)}, s32[112,2]{0,1:T(2,128)}, u32[]{:S(2)}) copy-start(s32[112,2]{0,1:T(2,128)} %param.34) | copy-start | bytes 2692
  57.7 53.3 %copy-start.4 = (f32[112,512]{1,0:T(8,128)S(1)}, f32[112,512]{1,0:T(8,128)}, u32[]{:S(2)}) copy-start(f32[112,512]{1,0:T(8,128)} %get-tuple-element.8) | copy-start | bytes 688132
